TPU v7x, 512 devices: a whole 4x8x8 slice. The times are simulated.
512 devices in a mesh: sp: 32 (over z, x), tp: 16 (over y, core).
Axes of the slice: x: 4, y: 8, z: 8, core: 2. Of those that a mesh axis runs over, the one named last changes fastest.
Arguments:
- residual_layer_input: bfloat16 [8192, 2048], P(('sp', 'tp')), may hold values from -6 to 6
- value_projected: bfloat16 [8192, 4096], P('sp', 'tp'), may hold values from -6 to 6
- key_projected: bfloat16 [8192, 2048], P('sp', 'tp'), may hold values from -6 to 6
- query_projected: bfloat16 [8192, 2048], P('sp', 'tp'), may hold values from -6 to 6
- output_gate_projected: bfloat16 [8192, 4096], P('sp', 'tp'), may hold values from -6 to 6
- step_projected_raw: bfloat16 [2, 8192, 64], P(None, 'sp', 'tp'), may hold values from -5.5 to 5
- head_decay_logarithm: float32 [2, 64], P(None, 'tp'), may hold values from -15 to -2.9
- position_extra_decay: float32 [8192, 64], P('sp', 'tp'), may hold values from -2.1 to 0
- value_filter_weight: bfloat16 [5, 4096], P(None, 'tp'), may hold values from -2.5 to 2.5
- key_filter_weight: bfloat16 [5, 2048], P(None, 'tp'), may hold values from -2.5 to 2.5
- query_filter_weight: bfloat16 [5, 2048], P(None, 'tp'), may hold values from -2.5 to 2.5
- head_norm_gain: float32 [4096], P('tp'), may hold values from 0.1 to 1.9
- mixer_output_matrix: bfloat16 [4096, 2048], P(None, 'tp'), may hold values from -0.09375 to 0.09375
- expert_norm_gain: float32 [2048], replicated, may hold values from 0.1 to 1.9
- routes: int32 [8192, 2], P('sp'), may hold values from 0 to 31, all different within a row; in each aligned block of 16 rows (0 to 15, 16 to 31, ...) at most 2 rows name the same one
- chosen_expert_weight: float32 [8192, 2], P(('sp', 'tp')), may hold values from 0.1 to 1
- expert_gate_matrix: bfloat16 [32, 2048, 4096], P('sp', None, 'tp'), may hold values from -0.125 to 0.125
- expert_up_matrix: bfloat16 [32, 2048, 4096], P('sp', None, 'tp'), may hold values from -0.125 to 0.125
- expert_down_matrix: bfloat16 [32, 4096, 2048], P('sp', 'tp'), may hold values from -0.09375 to 0.09375
Outputs:
- layer_output: bfloat16 [8192, 2048], P(('sp', 'tp'))
Inputs may be any that keep to these rules, and one draw needn't show every extreme that they name: `routes`: each row names 2 different experts; the rows of one device (aligned blocks of 16 rows) name one expert 2 times at most, and that most is reached.
All inputs are finite; a program needn't handle non-finite values.
Results may differ from a plain program's by a relative error of at most 0.015.
Values may be sent and summed in bfloat16 or wider, within the bound.
A program may use at most 64 MiB of HBM per device.

v0:
```python
import jax
import jax.numpy as jnp
from jax import lax
from jax.sharding import Mesh
from jax.sharding import PartitionSpec as P

HEAD_DIM = 64
STATE = 128
BLOCK = 128
TAPS = 5
SP = ("sp_0", "sp_1")
TP = ("tp_0", "tp_1")
SP_TP = ("sp_0", "sp_1", "tp_0", "tp_1")
epsilon = 1e-06


def padded_2(cells, sides, width):
    for axis, dim in sides:
        count = lax.axis_size(axis)
        ends = count - 1
        head = lax.slice_in_dim(cells, 0, width, axis=dim)
        tail = lax.slice_in_dim(cells, cells.shape[dim] - width, cells.shape[dim], axis=dim)
        cells = jnp.concatenate(
            [
                lax.ppermute(tail, axis, [(i, (i + 1) % count) for i in range(ends)]),
                cells,
                lax.ppermute(head, axis, [((i + 1) % count, i) for i in range(ends)]),
            ],
            axis=dim,
        )
    return cells


def filled_with(x, identity):
    return jax.tree.map(
        lambda part, zero: jnp.zeros_like(part) + jnp.asarray(zero, part.dtype), x, identity
    )


def carried_in(x, axes, combine, identity, reverse):
    before = start = filled_with(x, identity)
    so_far = x
    for axis in reversed(axes):
        count, here = (lax.axis_size(axis), lax.axis_index(axis))
        pieces = jax.tree.map(
            lambda part, kind: lax.all_gather(part.astype(kind), axis),
            so_far,
            (jnp.bfloat16, jnp.bfloat16),
        )
        inside, so_far = (start, start)
        for k in reversed(range(count)) if reverse else range(count):
            passed = k > here if reverse else k < here
            so_far = combine(
                so_far, jax.tree.map(lambda part, own: part[k].astype(own.dtype), pieces, x)
            )
            inside = jax.tree.map(lambda new, old: jnp.where(passed, new, old), so_far, inside)
        before = combine(inside, before)
    return before


def gather_axes(x, axes, dim):
    filled = x
    for number in range(len(axes) - 1, -1, -1):
        filled = lax.all_gather(filled, axes[number], axis=dim, tiled=True)
    return filled


def prefix_matrix(length):
    row_index = lax.broadcasted_iota(jnp.int32, (length, length), 0)
    column_index = lax.broadcasted_iota(jnp.int32, (length, length), 1)
    return (column_index <= row_index).astype(jnp.float32)


def carry_combine(first_part, second_part):
    return (
        first_part[0] + second_part[0],
        jnp.exp(second_part[0])[..., None, None] * first_part[1] + second_part[1],
    )


def local_chain(states, totals, reverse):

    def advance(carried, operands):
        block_state, block_total = operands
        return (jnp.exp(block_total)[..., None, None] * carried + block_state, carried)

    start_state = jnp.zeros(states.shape[1:], jnp.float32)
    return lax.scan(advance, start_state, (states, totals), reverse=reverse)


def mix_tokens(
    value_projected,
    key_projected,
    query_projected,
    output_gate_projected,
    step_projected_raw,
    head_decay_logarithm,
    position_extra_decay,
    value_filter_weight,
    key_filter_weight,
    query_filter_weight,
    head_norm_gain,
):
    tokens = value_projected.shape[0]
    value_width = value_projected.shape[1]
    key_width = key_projected.shape[1]
    head_count = step_projected_raw.shape[2]
    group_count = key_width // STATE
    per_group = head_count // group_count
    blocks = tokens // BLOCK
    joined = jnp.concatenate([value_projected, key_projected, query_projected], axis=1)
    padded = padded_2(joined, ((SP, 0),), (TAPS - 1) // 2).astype(jnp.float32)
    weights = jnp.concatenate(
        [value_filter_weight, key_filter_weight, query_filter_weight], axis=1
    ).astype(jnp.float32)
    filtered = weights[0] * padded[0:tokens]
    for offset in range(1, TAPS):
        filtered = filtered + weights[offset] * padded[offset : offset + tokens]
    values = filtered[:, :value_width].astype(jnp.bfloat16)
    key_rows = jax.nn.silu(filtered[:, value_width : value_width + key_width]).astype(jnp.bfloat16)
    key_rows = key_rows.reshape(blocks, BLOCK, group_count, STATE)
    query_rows = jax.nn.silu(filtered[:, value_width + key_width :]).astype(jnp.bfloat16)
    query_rows = query_rows.reshape(blocks, BLOCK, group_count, STATE)
    positive_step_sizes = jax.nn.softplus(step_projected_raw.astype(jnp.float32))
    decay_logarithm = (
        -jnp.exp(head_decay_logarithm)[:, None, :] * positive_step_sizes
        + position_extra_decay[None]
    )
    scaled = (
        values.astype(jnp.float32).reshape(tokens, head_count, HEAD_DIM)[None]
        * positive_step_sizes[..., None]
    ).astype(jnp.bfloat16)
    scaled = scaled.reshape(2, blocks, BLOCK, group_count, per_group, HEAD_DIM)
    log_blocks = decay_logarithm.reshape(2, blocks, BLOCK, group_count, per_group)
    running = jnp.einsum("ls,dbsgh->dblgh", prefix_matrix(BLOCK), log_blocks)
    forward_cum = running[0]
    backward_excl = running[1] - log_blocks[1]
    forward_total = running[0][:, -1]
    backward_total = running[1][:, -1]
    scores = jnp.einsum("blgn,bsgn->blsg", query_rows, key_rows, preferred_element_type=jnp.float32)
    position = lax.broadcasted_iota(jnp.int32, (BLOCK,), 0)
    lower_mask = (position[None, :] <= position[:, None])[None, :, :, None, None]
    upper_mask = (position[None, :] >= position[:, None])[None, :, :, None, None]
    forward_gap = jnp.where(lower_mask, forward_cum[:, :, None] - forward_cum[:, None, :], -jnp.inf)
    backward_gap = jnp.where(
        upper_mask, backward_excl[:, None, :] - backward_excl[:, :, None], -jnp.inf
    )
    forward_weight = (scores[..., None] * jnp.exp(forward_gap)).astype(jnp.bfloat16)
    backward_weight = (scores[..., None] * jnp.exp(backward_gap)).astype(jnp.bfloat16)
    inner = jnp.einsum(
        "blsgh,bsghp->blghp", forward_weight, scaled[0], preferred_element_type=jnp.float32
    )
    inner = inner + jnp.einsum(
        "blsgh,bsghp->blghp", backward_weight, scaled[1], preferred_element_type=jnp.float32
    )
    key_wide = key_rows.astype(jnp.float32)[:, :, :, None, :]
    forward_keys = (jnp.exp(forward_total[:, None] - forward_cum)[..., None] * key_wide).astype(
        jnp.bfloat16
    )
    backward_keys = (jnp.exp(backward_excl)[..., None] * key_wide).astype(jnp.bfloat16)
    forward_state = jnp.einsum(
        "bsghn,bsghp->bghpn", forward_keys, scaled[0], preferred_element_type=jnp.float32
    )
    backward_state = jnp.einsum(
        "bsghn,bsghp->bghpn", backward_keys, scaled[1], preferred_element_type=jnp.float32
    )
    forward_final, forward_before = local_chain(forward_state, forward_total, False)
    backward_final, backward_before = local_chain(backward_state, backward_total, True)
    forward_sum = jnp.sum(forward_total, axis=0)
    backward_sum = jnp.sum(backward_total, axis=0)
    zero_total = jnp.zeros(forward_sum.shape, jnp.float32)
    zero_state = jnp.zeros(forward_final.shape, jnp.float32)
    entering = carried_in(
        (forward_sum, forward_final), SP, carry_combine, (zero_total, zero_state), False
    )[1]
    leaving = carried_in(
        (backward_sum, backward_final), SP, carry_combine, (zero_total, zero_state), True
    )[1]
    forward_prior = jnp.cumsum(forward_total, axis=0) - forward_total
    backward_after = backward_sum[None] - jnp.cumsum(backward_total, axis=0)
    forward_in = jnp.exp(forward_prior)[..., None, None] * entering[None] + forward_before
    backward_in = jnp.exp(backward_after)[..., None, None] * leaving[None] + backward_before
    forward_read = jnp.exp(forward_cum)[..., None] * jnp.einsum(
        "blgn,bghpn->blghp",
        query_rows,
        forward_in.astype(jnp.bfloat16),
        preferred_element_type=jnp.float32,
    )
    backward_read = jnp.exp(backward_total[:, None] - backward_excl)[..., None] * jnp.einsum(
        "blgn,bghpn->blghp",
        query_rows,
        backward_in.astype(jnp.bfloat16),
        preferred_element_type=jnp.float32,
    )
    mixer_raw = (inner + forward_read + backward_read).reshape(tokens, head_count, HEAD_DIM)
    gated = mixer_raw * jax.nn.silu(output_gate_projected.astype(jnp.float32)).reshape(
        tokens, head_count, HEAD_DIM
    )
    inverse_rms = lax.rsqrt(jnp.mean(gated * gated, axis=-1, keepdims=True) + epsilon)
    head_normed = (gated * inverse_rms * head_norm_gain.reshape(head_count, HEAD_DIM)).astype(
        jnp.bfloat16
    )
    return head_normed.reshape(tokens, head_count * HEAD_DIM)


def slot_table(route_rows, experts, capacity):
    flat_ids = route_rows.reshape(-1)
    expert_ids = lax.broadcasted_iota(jnp.int32, (flat_ids.shape[0], experts), 1)
    matches = (flat_ids[:, None] == expert_ids).astype(jnp.int32)
    earlier = jnp.cumsum(matches, axis=0) - matches
    rank_in = jnp.sum(matches * earlier, axis=1)
    return (flat_ids * capacity + rank_in).reshape(route_rows.shape)


def dispatch_rows(slots, token_rows, places):
    place_ids = lax.broadcasted_iota(jnp.int32, (places,) + slots.shape, 0)
    one_hot = jnp.sum((place_ids == slots[None]).astype(jnp.float32), axis=2).astype(jnp.bfloat16)
    return jnp.dot(one_hot, token_rows, preferred_element_type=jnp.float32).astype(jnp.bfloat16)


def shards(
    residual_layer_input,
    value_projected,
    key_projected,
    query_projected,
    output_gate_projected,
    step_projected_raw,
    head_decay_logarithm,
    position_extra_decay,
    value_filter_weight,
    key_filter_weight,
    query_filter_weight,
    head_norm_gain,
    mixer_output_matrix,
    expert_norm_gain,
    routes,
    chosen_expert_weight,
    expert_gate_matrix,
    expert_up_matrix,
    expert_down_matrix,
):
    heads_out = mix_tokens(
        value_projected,
        key_projected,
        query_projected,
        output_gate_projected,
        step_projected_raw,
        head_decay_logarithm,
        position_extra_decay,
        value_filter_weight,
        key_filter_weight,
        query_filter_weight,
        head_norm_gain,
    )
    projected = jnp.dot(
        gather_axes(heads_out, TP, 1), mixer_output_matrix, preferred_element_type=jnp.float32
    ).astype(jnp.bfloat16)
    mixer_out = lax.all_to_all(projected, TP, split_axis=0, concat_axis=1, tiled=True)
    middle = (residual_layer_input.astype(jnp.float32) + mixer_out.astype(jnp.float32)).astype(
        jnp.bfloat16
    )
    residual = middle.astype(jnp.float32)
    normed = (
        residual
        * lax.rsqrt(jnp.mean(residual * residual, axis=-1, keepdims=True) + epsilon)
        * expert_norm_gain
    ).astype(jnp.bfloat16)
    own_rows = normed.shape[0]
    model_width = normed.shape[1]
    top_count = routes.shape[1]
    experts = lax.axis_size(SP)
    capacity = 2 * own_rows * top_count // experts
    places = experts * capacity
    position = lax.axis_index(TP)
    own_routes = lax.dynamic_slice_in_dim(routes, position * own_rows, own_rows, 0)
    own_slots = slot_table(own_routes, experts, capacity)
    outgoing = dispatch_rows(own_slots, normed, places)
    received = lax.all_to_all(
        outgoing.reshape(experts, capacity, model_width),
        SP,
        split_axis=0,
        concat_axis=0,
        tiled=True,
    )
    arrived = lax.all_gather(received[None], TP, axis=0, tiled=True)
    slot_rows = arrived.reshape(-1, model_width)
    gate_value = jnp.dot(slot_rows, expert_gate_matrix[0], preferred_element_type=jnp.float32)
    up_value = jnp.dot(slot_rows, expert_up_matrix[0], preferred_element_type=jnp.float32)
    hidden = (jax.nn.silu(gate_value) * up_value).astype(jnp.bfloat16)
    partial_sum = jnp.dot(hidden, expert_down_matrix[0], preferred_element_type=jnp.float32).astype(
        jnp.bfloat16
    )
    summed = lax.psum_scatter(
        partial_sum.astype(jnp.float32).reshape(arrived.shape).astype(jnp.bfloat16),
        TP,
        scatter_dimension=0,
        tiled=True,
    )
    results = summed.reshape(experts, capacity, model_width)
    returned = lax.all_to_all(results, SP, split_axis=0, concat_axis=0, tiled=True)
    chosen = (
        lax.broadcasted_iota(jnp.int32, (own_rows, top_count, places), 2) == own_slots[:, :, None]
    )
    mixing = jnp.sum(jnp.where(chosen, chosen_expert_weight[:, :, None], 0.0), axis=1)
    expert_mix = jnp.dot(mixing, returned.reshape(places, model_width).astype(jnp.float32))
    return (residual + expert_mix).astype(jnp.bfloat16)


def solution(mesh):
    finer = Mesh(mesh.devices.reshape(8, 4, 8, 2), ("sp_0", "sp_1", "tp_0", "tp_1"))
    return jax.shard_map(
        shards,
        mesh=finer,
        in_specs=(
            P(SP_TP, None),
            P(SP, TP),
            P(SP, TP),
            P(SP, TP),
            P(SP, TP),
            P(None, SP, TP),
            P(None, TP),
            P(SP, TP),
            P(None, TP),
            P(None, TP),
            P(None, TP),
            P(TP),
            P(None, TP),
            P(),
            P(SP, None),
            P(SP_TP, None),
            P(SP, None, TP),
            P(SP, None, TP),
            P(SP, TP, None),
        ),
        out_specs=P(SP_TP, None),
        check_vma=False,
    )
```

profile of v0, /device:TPU:25, one launch (start us, length us, event | category | flops | bytes accessed | tf_op | source)
XLA Modules:
  0.0 411.3 jit_solution(13802664168214537956)
XLA Ops:
  6.5 1.1 copy.131
  7.6 0.9 copy.132
  8.6 0.9 copy.133
  9.7 3.1 collective-permute-start
  12.8 1.3 collective-permute-start.1
  14.1 0.6 iota_compare_fusion.1
  14.7 0.6 iota_compare_fusion
  15.3 0.7 exponential_negate_fusion
  16.0 0.8 compare_select_fusion
  16.9 0.6 slice_bitcast_fusion.11
  17.8 1.3 dynamic-slice
  19.7 0.2 dynamic-update-slice.1
  20.2 9.9 %all-reduce.2 = (bf16[16]{0:T(256)(128)(2,1)S(1)}, bf16[16]{0:T(256)(128)(2,1)S(1)}) all-reduce(bf16[16]{0:T(256)(128)(2,1)S(1)} %dynamic-update-slice.1, bf16[16]{0:T(256)(128)(2,1)S(1)} %dynamic-update-slice), channel_id=4, replica_groups=mesh['sp_0'=8,'sp_1'=4,'tp_0'=8,'tp_1'=2] {'sp_1'}, use_global_device_ids=true, to_apply=%add.1 | all-reduce | flops 32 | bytes 128
  30.1 18.0 %all_gather.46 = bf16[8,1,4]{2,1,0:T(2,128)(2,1)S(1)} all-gather(bf16[1,1,4]{2,1,0:T(2,128)(2,1)S(1)} %get-tuple-element.265), channel_id=1, replica_groups=mesh['sp_0'=8,'sp_1'=4,'tp_0'=8,'tp_1'=2] {'sp_0'}, dimensions={0}, use_global_device_ids=true | all-gather | bytes 72 | tf_op jit(solution)/shard_map/all_gather | solution.py:46
  48.1 0.6 fusion.131
  48.8 9.8 %all_gather.51 = bf16[8,1,4]{2,1,0:T(2,128)(2,1)S(1)} all-gather(bf16[1,1,4]{2,1,0:T(2,128)(2,1)S(1)} %get-tuple-element.269), channel_id=1, replica_groups=mesh['sp_0'=8,'sp_1'=4,'tp_0'=8,'tp_1'=2] {'sp_0'}, dimensions={0}, use_global_device_ids=true | all-gather | bytes 72 | tf_op jit(solution)/shard_map/all_gather | solution.py:46
  58.6 0.6 fusion.114
  59.4 0.6 subtract_exponential_fusion.2
  60.0 0.6 subtract_exponential_fusion.3
  60.6 1.0 copy.150
  61.7 0.7 fusion.132
  62.4 0.7 fusion.133
  63.0 0.9 maximum_convert_fusion.4
  64.4 0.9 fusion.21
  65.5 0.7 reshape.1004
  66.7 0.4 convolution_bitcast_fusion.1
  67.2 0.3 while.30
  67.6 9.4 %all-gather.1 = bf16[4,4,64,128]{3,2,1,0:T(8,128)(2,1)S(1)} all-gather(bf16[1,4,64,128]{3,2,1,0:T(8,128)(2,1)S(1)} %convert_element_type.652), channel_id=3, replica_groups=mesh['sp_0'=8,'sp_1'=4,'tp_0'=8,'tp_1'=2] {'sp_1'}, dimensions={0}, use_global_device_ids=true | all-gather | bytes 327680 | tf_op jit(solution)/shard_map/all_gather | solution.py:46
  77.1 19.1 %all_gather.49 = bf16[8,1,4,64,128]{4,3,2,1,0:T(8,128)(2,1)S(1)} all-gather(bf16[1,1,4,64,128]{4,3,2,1,0:T(8,128)(2,1)S(1)} %fusion.75), channel_id=1, replica_groups=mesh['sp_0'=8,'sp_1'=4,'tp_0'=8,'tp_1'=2] {'sp_0'}, dimensions={0}, use_global_device_ids=true | all-gather | bytes 589824 | tf_op jit(solution)/shard_map/all_gather | solution.py:46
  96.2 0.4 convolution_bitcast_fusion
  96.6 1.5 while.31
  96.7 0.6 fusion.161
  97.4 0.6 fusion.161
  98.2 9.7 %all-gather.3 = bf16[4,4,64,128]{3,2,1,0:T(8,128)(2,1)S(1)} all-gather(bf16[1,4,64,128]{3,2,1,0:T(8,128)(2,1)S(1)} %convert_element_type.683), channel_id=5, replica_groups=mesh['sp_0'=8,'sp_1'=4,'tp_0'=8,'tp_1'=2] {'sp_1'}, dimensions={0}, use_global_device_ids=true | all-gather | bytes 327680 | tf_op jit(solution)/shard_map/all_gather | solution.py:46
  108.0 19.3 %all_gather.54 = bf16[8,1,4,64,128]{4,3,2,1,0:T(8,128)(2,1)S(1)} all-gather(bf16[1,1,4,64,128]{4,3,2,1,0:T(8,128)(2,1)S(1)} %fusion.72), channel_id=1, replica_groups=mesh['sp_0'=8,'sp_1'=4,'tp_0'=8,'tp_1'=2] {'sp_0'}, dimensions={0}, use_global_device_ids=true | all-gather | bytes 589824 | tf_op jit(solution)/shard_map/all_gather | solution.py:46
  127.3 1.0 copy.159
  128.2 0.8 copy.136
  129.0 1.3 fusion.29
  130.3 1.3 fusion.6
  131.7 1.1 fusion.63
  132.8 0.9 fusion.10
  133.7 1.1 fusion.70
  134.8 1.2 fusion.34
  136.2 0.8 fusion.32
  137.0 30.0 %all_gather.55 = bf16[256,512]{0,1:T(8,128)(2,1)} all-gather(bf16[256,256]{0,1:T(8,128)(2,1)S(1)} %fusion.32), channel_id=1, replica_groups=mesh['sp_0'=8,'sp_1'=4,'tp_0'=8,'tp_1'=2] {'tp_1'}, dimensions={1}, use_global_device_ids=true | all-gather | bytes 393216 | tf_op jit(solution)/shard_map/all_gather | solution.py:64
  167.1 0.8 constant_dynamic-slice_fusion.2
  168.4 33.5 %all-gather.8.cloned.1.call-done = bf16[256,4096]{0,1:T(8,128)(2,1)} async-done(((bf16[256,512]{0,1:T(8,128)(2,1)}), bf16[256,4096]{0,1:T(8,128)(2,1)}) %all-gather.8.cloned.1.call-update) | async-done | bytes 2097168 | tf_op jit(solution)/shard_map/all_gather | solution.py:64
  201.9 3.2 convolution_convert_fusion.2
  205.1 10.1 %all-to-all-start = ((bf16[16,16,128]{2,1,0:T(8,128)(2,1)}), bf16[16,16,128]{2,1,0:T(8,128)(2,1)S(1)}, u32[]{:S(2)}, u32[]{:S(2)}) async-start(bf16[16,16,128]{2,1,0:T(8,128)(2,1)} %bitcast.67), calls=%async_computation | async-start | bytes 131072 | tf_op jit(solution)/shard_map/all_to_all | solution.py:258
  215.4 4.7 %all-to-all-done = bf16[16,16,128]{2,1,0:T(8,128)(2,1)S(1)} async-done(((bf16[16,16,128]{2,1,0:T(8,128)(2,1)}), bf16[16,16,128]{2,1,0:T(8,128)(2,1)S(1)}, u32[]{:S(2)}, u32[]{:S(2)}) %all-to-all-start) | async-done | bytes 65568 | tf_op jit(solution)/shard_map/all_to_all | solution.py:258
  220.3 0.3 convolution_convert_fusion.1
  220.8 21.4 %all_to_all.23 = bf16[32,2,2048]{2,1,0:T(2,128)(2,1)} all-to-all(bf16[32,2,2048]{2,1,0:T(2,128)(2,1)S(1)} %reshape.1011), channel_id=1, replica_groups=mesh['sp_0'=8,'sp_1'=4,'tp_0'=8,'tp_1'=2] {'sp_0','sp_1'}, dimensions={0} | all-to-all | bytes 524288 | tf_op jit(solution)/shard_map/all_to_all | solution.py:278
  242.2 0.2 reduce-scatter.2.cloned.1.call-start
  242.4 38.9 %all-gather.10.cloned.1.call-done = bf16[512,2,2048]{2,1,0:T(2,128)(2,1)} async-done(((bf16[32,2,2048]{2,1,0:T(2,128)(2,1)}), bf16[512,2,2048]{2,1,0:T(2,128)(2,1)}) %all-gather.10.cloned.1.call-update) | async-done | bytes 4194320 | tf_op jit(solution)/shard_map/all_gather | solution.py:285
  281.3 7.2 %reshape.1012 = bf16[1024,2048]{1,0:T(8,128)(2,1)} reshape(bf16[512,2,2048]{2,1,0:T(2,128)(2,1)} %all-gather.10.cloned.1.call-done) | data formatting | bytes 8388608 | tf_op jit(solution)/shard_map/reshape | solution.py:286
  288.5 4.5 %fusion.14 = f32[1024,256]{1,0:T(8,128)} fusion(bf16[1024,2048]{1,0:T(8,128)(2,1)} %reshape.1012, bf16[1,2048,256]{2,1,0:T(8,128)(2,1)S(1)} %copy-done.16), kind=kOutput, calls=%fused_computation.31 | convolution fusion | flops 1073741824 | bytes 6291456 | tf_op jit(solution)/shard_map/dot_general | solution.py:287
  293.0 9.1 %convolution_convert_fusion = bf16[1024,2048]{1,0:T(8,128)(2,1)} fusion(bf16[1024,2048]{1,0:T(8,128)(2,1)} %reshape.1012, bf16[1,256,2048]{2,1,0:T(8,128)(2,1)S(1)} %copy-done, bf16[1,2048,256]{2,1,0:T(8,128)(2,1)} %param.40, f32[1024,256]{1,0:T(8,128)} %fusion.14), kind=kOutput, calls=%fused_computation.10 | convolution fusion | flops 2151153664 | bytes 11534336 | tf_op jit(solution)/shard_map/dot_general | solution.py:290
  302.1 7.6 %convert_element_type.713 = bf16[16,32,2,2048]{3,2,1,0:T(2,128)(2,1)} reshape(bf16[1024,2048]{1,0:T(8,128)(2,1)} %convolution_convert_fusion) | data formatting | bytes 8388608 | tf_op jit(solution)/shard_map/convert_element_type | solution.py:294
  309.8 6.1 %copy.156 = bf16[16,32,2,2048]{3,1,2,0:T(8,128)(2,1)} copy(bf16[16,32,2,2048]{3,2,1,0:T(2,128)(2,1)} %convert_element_type.713) | data formatting | bytes 8388608 | tf_op jit(solution)/shard_map/convert_element_type | solution.py:294
  315.8 64.9 %reduce-scatter.2.cloned.1.call-done = bf16[1,32,2,2048]{3,1,2,0:T(8,128)(2,1)} async-done(((bf16[16,32,2,2048]{3,1,2,0:T(8,128)(2,1)}), bf16[1,32,2,2048]{3,1,2,0:T(8,128)(2,1)}) %reduce-scatter.2.cloned.1.call-update) | async-done | bytes 262160 | tf_op jit(solution)/shard_map/reduce_scatter | solution.py:293
  380.8 1.9 copy.157
  382.7 10.1 %all-to-all-start.2 = ((bf16[32,2,2048]{2,1,0:T(2,128)(2,1)}), bf16[32,2,2048]{2,1,0:T(2,128)(2,1)S(1)}, u32[]{:S(2)}, u32[]{:S(2)}) async-start(bf16[32,2,2048]{2,1,0:T(2,128)(2,1)} %copy.157), calls=%async_computation.3 | async-start | bytes 524288 | tf_op jit(solution)/shard_map/all_to_all | solution.py:300
  392.8 11.1 %all-to-all-done.2 = bf16[32,2,2048]{2,1,0:T(2,128)(2,1)S(1)} async-done(((bf16[32,2,2048]{2,1,0:T(2,128)(2,1)}), bf16[32,2,2048]{2,1,0:T(2,128)(2,1)S(1)}, u32[]{:S(2)}, u32[]{:S(2)}) %all-to-all-start.2) | async-done | bytes 262176 | tf_op jit(solution)/shard_map/all_to_all | solution.py:300
  404.0 0.8 fusion.4
  (102 shorter events, 4.5 us)
Async XLA Ops:
  6.5 286.5 %copy-start = (bf16[1,256,2048]{2,1,0:T(8,128)(2,1)S(1)}, bf16[1,256,2048]{2,1,0:T(8,128)(2,1)}, u32[]{:S(2)}) copy-start(bf16[1,256,2048]{2,1,0:T(8,128)(2,1)} %param.41) | copy-start | bytes 3145732
  6.5 195.4 %all-gather.8.cloned.1.call-start = ((), (), s32[]{:S(2)}) async-start(), calls=%async_computation.4 | async-start | bytes 2359296 | tf_op jit(solution)/shard_map/all_gather | solution.py:64
  9.7 54.5 %collective-permute-start = (bf16[2,512]{0,1:T(8,128)(2,1)S(1)}, bf16[2,512]{0,1:T(8,128)(2,1)S(1)}, u32[]{:S(2)}, u32[]{:S(2)}) collective-permute-start(bf16[2,512]{0,1:T(8,128)(2,1)S(1)} %get-tuple-element.275), channel_id=1, source_target_pairs={{0,16},{16,32},{32,48},{48,64},{64,80},{80,96},{96,112},{112,128},... | collective-permute-start | bytes 6152 | tf_op jit(solution)/shard_map/ppermute | solution.py:25
  12.8 51.4 %collective-permute-start.1 = (bf16[2,512]{0,1:T(8,128)(2,1)S(1)}, bf16[2,512]{0,1:T(8,128)(2,1)S(1)}, u32[]{:S(2)}, u32[]{:S(2)}) collective-permute-start(bf16[2,512]{0,1:T(8,128)(2,1)S(1)} %get-tuple-element.276), channel_id=1, source_target_pairs={{16,0},{32,16},{48,32},{64,48},{80,64},{96,80},{112,96},{128,112},... | collective-permute-start | bytes 6152 | tf_op jit(solution)/shard_map/ppermute | solution.py:27
  17.8 46.3 %copy-start.5 = (f32[2,4]{1,0:T(2,128)}, f32[2,4]{1,0:T(2,128)S(1)}, u32[]{:S(2)}) copy-start(f32[2,4]{1,0:T(2,128)S(1)} %get-tuple-element.240) | copy-start | bytes 100
  62.3 14.6 %copy-start.7 = (f32[4]{0:T(128)}, f32[4]{0:T(128)S(1)}, u32[]{:S(2)}) copy-start(f32[4]{0:T(128)S(1)} %get-tuple-element.308) | copy-start | bytes 52
  62.3 14.6 %copy-start.8 = (f32[4]{0:T(128)}, f32[4]{0:T(128)S(1)}, u32[]{:S(2)}) copy-start(f32[4]{0:T(128)S(1)} %get-tuple-element.309) | copy-start | bytes 52
  62.3 14.6 %copy-start.9 = (f32[4]{0:T(128)}, f32[4]{0:T(128)S(1)}, u32[]{:S(2)}) copy-start(f32[4]{0:T(128)S(1)} %get-tuple-element.310) | copy-start | bytes 52
  62.3 14.6 %copy-start.10 = (f32[4]{0:T(128)}, f32[4]{0:T(128)S(1)}, u32[]{:S(2)}) copy-start(f32[4]{0:T(128)S(1)} %get-tuple-element.311) | copy-start | bytes 52
  66.5 0.6 copy-start.2
  67.2 40.6 %copy-start.11 = (f32[4]{0:T(128)S(1)}, f32[4]{0:T(128)}, u32[]{:S(2)}) copy-start(f32[4]{0:T(128)} %get-tuple-element.313) | copy-start | bytes 52
  67.2 40.6 %copy-start.12 = (f32[4]{0:T(128)S(1)}, f32[4]{0:T(128)}, u32[]{:S(2)}) copy-start(f32[4]{0:T(128)} %get-tuple-element.314) | copy-start | bytes 52
  67.2 40.6 %copy-start.13 = (f32[4]{0:T(128)S(1)}, f32[4]{0:T(128)}, u32[]{:S(2)}) copy-start(f32[4]{0:T(128)} %get-tuple-element.315) | copy-start | bytes 52
  67.2 40.6 %copy-start.14 = (f32[4]{0:T(128)S(1)}, f32[4]{0:T(128)}, u32[]{:S(2)}) copy-start(f32[4]{0:T(128)} %get-tuple-element.316) | copy-start | bytes 52
  67.5 29.1 %copy-start.1 = (f32[2,1,4,64,128]{4,3,2,1,0:T(8,128)}, f32[2,1,4,64,128]{4,3,2,1,0:T(8,128)S(1)}, u32[]{:S(2)}) copy-start(f32[2,1,4,64,128]{4,3,2,1,0:T(8,128)S(1)} %get-tuple-element.138) | copy-start | bytes 786436
  96.2 11.6 %copy-start.3 = (bf16[2,128,4,64]{1,0,3,2:T(2,128)(2,1)}, bf16[2,128,4,64]{1,0,3,2:T(2,128)(2,1)S(1)}, u32[]{:S(2)}) copy-start(bf16[2,128,4,64]{1,0,3,2:T(2,128)(2,1)S(1)} %reshape.1006) | copy-start | bytes 393220
  132.7 87.4 %copy-start.4 = (bf16[16,2048]{1,0:T(8,128)(2,1)S(1)}, bf16[16,2048]{1,0:T(8,128)(2,1)}, u32[]{:S(2)}) copy-start(bf16[16,2048]{1,0:T(8,128)(2,1)} %param.23) | copy-start | bytes 196612
  132.8 87.5 %copy-start.6 = (f32[2048]{0:T(1024)S(1)}, f32[2048]{0:T(1024)}, u32[]{:S(2)}) copy-start(f32[2048]{0:T(1024)} %param.36) | copy-start | bytes 24580
  205.1 15.0 %all-to-all-start = ((bf16[16,16,128]{2,1,0:T(8,128)(2,1)}), bf16[16,16,128]{2,1,0:T(8,128)(2,1)S(1)}, u32[]{:S(2)}, u32[]{:S(2)}) async-start(bf16[16,16,128]{2,1,0:T(8,128)(2,1)} %bitcast.67), calls=%async_computation | async-start | bytes 131072 | tf_op jit(solution)/shard_map/all_to_all | solution.py:258
  215.2 66.2 %all-gather.10.cloned.1.call-start = ((), (), s32[]{:S(2)}) async-start(), calls=%async_computation.6 | async-start | bytes 4456448 | tf_op jit(solution)/shard_map/all_gather | solution.py:285
  242.2 46.4 %copy-start.16 = (bf16[1,2048,256]{2,1,0:T(8,128)(2,1)S(1)}, bf16[1,2048,256]{2,1,0:T(8,128)(2,1)}, u32[]{:S(2)}) copy-start(bf16[1,2048,256]{2,1,0:T(8,128)(2,1)} %param.39) | copy-start | bytes 3145732
  242.2 138.6 %reduce-scatter.2.cloned.1.call-start = ((), (), s32[]{:S(2)}) async-start(), calls=%async_computation.5 | async-start | bytes 4456448 | tf_op jit(solution)/shard_map/reduce_scatter | solution.py:293
  315.8 76.9 %copy-start.15 = (f32[16,2]{0,1:T(2,128)S(1)}, f32[16,2]{0,1:T(2,128)}, u32[]{:S(2)}) copy-start(f32[16,2]{0,1:T(2,128)} %param.38) | copy-start | bytes 388
  382.7 21.2 %all-to-all-start.2 = ((bf16[32,2,2048]{2,1,0:T(2,128)(2,1)}), bf16[32,2,2048]{2,1,0:T(2,128)(2,1)S(1)}, u32[]{:S(2)}, u32[]{:S(2)}) async-start(bf16[32,2,2048]{2,1,0:T(2,128)(2,1)} %copy.157), calls=%async_computation.3 | async-start | bytes 524288 | tf_op jit(solution)/shard_map/all_to_all | solution.py:300
Sparse Core Ops, SparseCore 0:
  167.2 34.6 all-gather.7
  242.3 39.0 all-gather.9
  316.0 64.7 reduce-scatter.1
where the time goes:
time: 413 us; the launch traced here: 411 us
  waiting for transfers between devices  153 us (37%)
  blocking collectives  147 us (36%)
  local copies, waits for them, and re-layouts  35.1 us (8%)
  starting transfers between devices  24.8 us (6%)
  matrix products  23.8 us (6%)
  between operations  14.4 us (3%)
  other arithmetic  13.5 us (3%)
    all_gather x6, blocking collectives, carried_in(): lax.all_gather(part.astype(kind), axis)  85.3 us
    reduce_scatter x1, waiting for transfers between devices, shards(): lax.psum_scatter(partial_sum.astype(jnp.float32).reshape(arrived.shape).a...  64.9 us
    all_gather x1, waiting for transfers between devices, shards(): arrived = lax.all_gather(received[None], TP, axis=0, tiled=True)  38.9 us
    all_gather x1, waiting for transfers between devices, gather_axes(): filled = lax.all_gather(filled, axes[number], axis=dim, tiled=True)  33.5 us
    all_gather x1, blocking collectives, gather_axes(): filled = lax.all_gather(filled, axes[number], axis=dim, tiled=True)  30 us
    all_to_all x1, blocking collectives, shards(): lax.all_to_all(outgoing.reshape(experts, capacity, model_width), SP, spli...  21.4 us
    convert_element_type x2, local copies, waits for them, and re-layouts, shards(): partial_sum.astype(jnp.float32).reshape(arrived.shape).astype(jnp.bfloat16)  13.7 us
    all_to_all x1, waiting for transfers between devices, shards(): lax.all_to_all(results, SP, split_axis=0, concat_axis=0, tiled=True)  11.1 us
  transfers between devices with their start and end apart: 7, of which 5 were waited for; matrix products, arithmetic and copies ran while one was open for 3% of the time, Pallas kernels for 0%

commit v1 on v0

--- a/solution.py
+++ b/solution.py
@@ -282,7 +282,9 @@
         concat_axis=0,
         tiled=True,
     )
-    arrived = lax.all_gather(received[None], TP, axis=0, tiled=True)
+    arrived = jnp.concatenate(
+        lax.all_to_all(jnp.stack([received[None]] * lax.axis_size(TP)), TP, 0, 0), axis=0
+    )
     slot_rows = arrived.reshape(-1, model_width)
     gate_value = jnp.dot(slot_rows, expert_gate_matrix[0], preferred_element_type=jnp.float32)
     up_value = jnp.dot(slot_rows, expert_up_matrix[0], preferred_element_type=jnp.float32)

time: 413 us -> 473 us (1.15)
  blocking collectives: 147 us -> 249 us
  waiting for transfers between devices: 153 us -> 108 us
    all_to_all x0 -> x1, blocking collectives: none -> 102 us  [shards(): lax.all_to_all(jnp.stack([received[None]] * lax.axis_size(TP)), TP, 0, 0)]
    all_gather x1 -> x0, waiting for transfers between devices: 38.9 us -> none  [shards(): arrived = lax.all_gather(received[None], TP, axis=0, tiled=True)]
    another operation x7 -> x9, local copies, waits for them, and re-layouts: 1.74 us -> 12.2 us  [the longest x1 7.27 us: shards(): slot_rows = arrived.reshape(-1, model_width)]
    reshape x1 -> x0, local copies, waits for them, and re-layouts: 7.19 us -> none  [shards(): slot_rows = arrived.reshape(-1, model_width)]
    reduce_scatter x1, waiting for transfers between devices: 64.9 us -> 58.6 us  [shards(): lax.psum_scatter(partial_sum.astype(jnp.float32).reshape(arrived.shape).a...]
  transfers between devices with their start and end apart: 7 -> 6, of which waited for: 5 -> 4; matrix products, arithmetic and copies ran while one was open for 3% -> 3% of each run, Pallas kernels for 0% -> 0%
where the time goes in v1:
time: 473 us; the launch traced here: 471 us
  blocking collectives  249 us (53%)
  waiting for transfers between devices  108 us (23%)
  local copies, waits for them, and re-layouts  38.4 us (8%)
  starting transfers between devices  24.4 us (5%)
  matrix products  23.8 us (5%)
  between operations  14.7 us (3%)
  other arithmetic  13.4 us (3%)
    all_to_all x1, blocking collectives, shards(): lax.all_to_all(jnp.stack([received[None]] * lax.axis_size(TP)), TP, 0, 0)  102 us
    all_gather x6, blocking collectives, carried_in(): lax.all_gather(part.astype(kind), axis)  85.2 us
    reduce_scatter x1, waiting for transfers between devices, shards(): lax.psum_scatter(partial_sum.astype(jnp.float32).reshape(arrived.shape).a...  58.6 us
    all_gather x1, waiting for transfers between devices, gather_axes(): filled = lax.all_gather(filled, axes[number], axis=dim, tiled=True)  33.5 us
    all_gather x1, blocking collectives, gather_axes(): filled = lax.all_gather(filled, axes[number], axis=dim, tiled=True)  30.1 us
    all_to_all x1, blocking collectives, shards(): lax.all_to_all(outgoing.reshape(experts, capacity, model_width), SP, spli...  21.3 us
    convert_element_type x2, local copies, waits for them, and re-layouts, shards(): partial_sum.astype(jnp.float32).reshape(arrived.shape).astype(jnp.bfloat16)  13.7 us
    all_to_all x1, waiting for transfers between devices, shards(): lax.all_to_all(results, SP, split_axis=0, concat_axis=0, tiled=True)  11.1 us
  transfers between devices with their start and end apart: 6, of which 4 were waited for; matrix products, arithmetic and copies ran while one was open for 3% of the time, Pallas kernels for 0%

profile of v1, /device:TPU:25, one launch (start us, length us, event | category | flops | bytes accessed | tf_op | source)
XLA Modules:
  0.0 471.4 jit_solution(9273919303022134508)
XLA Ops:
  6.5 1.1 copy.131
  7.6 0.9 copy.132
  8.6 0.9 copy.133
  9.7 3.1 collective-permute-start
  12.8 1.3 collective-permute-start.1
  14.1 0.6 iota_compare_fusion.1
  14.7 0.6 iota_compare_fusion
  15.3 0.7 exponential_negate_fusion
  16.0 0.8 compare_select_fusion
  16.9 0.6 slice_bitcast_fusion.11
  17.8 1.3 dynamic-slice
  19.7 0.2 dynamic-update-slice.1
  20.2 9.9 %all-reduce.2 = (bf16[16]{0:T(256)(128)(2,1)S(1)}, bf16[16]{0:T(256)(128)(2,1)S(1)}) all-reduce(bf16[16]{0:T(256)(128)(2,1)S(1)} %dynamic-update-slice.1, bf16[16]{0:T(256)(128)(2,1)S(1)} %dynamic-update-slice), channel_id=4, replica_groups=mesh['sp_0'=8,'sp_1'=4,'tp_0'=8,'tp_1'=2] {'sp_1'}, use_global_device_ids=true, to_apply=%add.1 | all-reduce | flops 32 | bytes 128
  30.1 18.0 %all_gather.43 = bf16[8,1,4]{2,1,0:T(2,128)(2,1)S(1)} all-gather(bf16[1,1,4]{2,1,0:T(2,128)(2,1)S(1)} %get-tuple-element.265), channel_id=1, replica_groups=mesh['sp_0'=8,'sp_1'=4,'tp_0'=8,'tp_1'=2] {'sp_0'}, dimensions={0}, use_global_device_ids=true | all-gather | bytes 72 | tf_op jit(solution)/shard_map/all_gather | solution.py:46
  48.2 0.6 fusion.131
  48.8 9.8 %all_gather.48 = bf16[8,1,4]{2,1,0:T(2,128)(2,1)S(1)} all-gather(bf16[1,1,4]{2,1,0:T(2,128)(2,1)S(1)} %get-tuple-element.269), channel_id=1, replica_groups=mesh['sp_0'=8,'sp_1'=4,'tp_0'=8,'tp_1'=2] {'sp_0'}, dimensions={0}, use_global_device_ids=true | all-gather | bytes 72 | tf_op jit(solution)/shard_map/all_gather | solution.py:46
  58.7 0.6 fusion.114
  59.4 0.6 subtract_exponential_fusion.2
  60.0 0.6 subtract_exponential_fusion.3
  60.6 1.0 copy.150
  61.7 0.7 fusion.132
  62.3 0.7 fusion.133
  63.0 0.9 maximum_convert_fusion.4
  64.4 0.9 fusion.21
  65.5 0.7 reshape.1003
  66.6 0.4 convolution_bitcast_fusion.1
  67.2 0.3 while.30
  67.6 9.4 %all-gather.1 = bf16[4,4,64,128]{3,2,1,0:T(8,128)(2,1)S(1)} all-gather(bf16[1,4,64,128]{3,2,1,0:T(8,128)(2,1)S(1)} %convert_element_type.652), channel_id=3, replica_groups=mesh['sp_0'=8,'sp_1'=4,'tp_0'=8,'tp_1'=2] {'sp_1'}, dimensions={0}, use_global_device_ids=true | all-gather | bytes 327680 | tf_op jit(solution)/shard_map/all_gather | solution.py:46
  77.1 19.1 %all_gather.46 = bf16[8,1,4,64,128]{4,3,2,1,0:T(8,128)(2,1)S(1)} all-gather(bf16[1,1,4,64,128]{4,3,2,1,0:T(8,128)(2,1)S(1)} %fusion.75), channel_id=1, replica_groups=mesh['sp_0'=8,'sp_1'=4,'tp_0'=8,'tp_1'=2] {'sp_0'}, dimensions={0}, use_global_device_ids=true | all-gather | bytes 589824 | tf_op jit(solution)/shard_map/all_gather | solution.py:46
  96.2 0.4 convolution_bitcast_fusion
  96.6 1.6 while.31
  96.6 0.7 fusion.161
  97.5 0.6 fusion.161
  98.2 9.7 %all-gather.3 = bf16[4,4,64,128]{3,2,1,0:T(8,128)(2,1)S(1)} all-gather(bf16[1,4,64,128]{3,2,1,0:T(8,128)(2,1)S(1)} %convert_element_type.683), channel_id=5, replica_groups=mesh['sp_0'=8,'sp_1'=4,'tp_0'=8,'tp_1'=2] {'sp_1'}, dimensions={0}, use_global_device_ids=true | all-gather | bytes 327680 | tf_op jit(solution)/shard_map/all_gather | solution.py:46
  108.0 19.3 %all_gather.51 = bf16[8,1,4,64,128]{4,3,2,1,0:T(8,128)(2,1)S(1)} all-gather(bf16[1,1,4,64,128]{4,3,2,1,0:T(8,128)(2,1)S(1)} %fusion.72), channel_id=1, replica_groups=mesh['sp_0'=8,'sp_1'=4,'tp_0'=8,'tp_1'=2] {'sp_0'}, dimensions={0}, use_global_device_ids=true | all-gather | bytes 589824 | tf_op jit(solution)/shard_map/all_gather | solution.py:46
  127.3 1.0 copy.159
  128.2 0.8 copy.136
  129.0 1.3 fusion.29
  130.3 1.3 fusion.6
  131.7 1.1 fusion.63
  132.8 0.9 fusion.10
  133.7 1.1 fusion.70
  134.8 1.2 fusion.34
  136.2 0.8 fusion.32
  137.0 30.1 %all_gather.52 = bf16[256,512]{0,1:T(8,128)(2,1)} all-gather(bf16[256,256]{0,1:T(8,128)(2,1)S(1)} %fusion.32), channel_id=1, replica_groups=mesh['sp_0'=8,'sp_1'=4,'tp_0'=8,'tp_1'=2] {'tp_1'}, dimensions={1}, use_global_device_ids=true | all-gather | bytes 393216 | tf_op jit(solution)/shard_map/all_gather | solution.py:64
  167.1 0.8 constant_dynamic-slice_fusion.2
  168.5 33.5 %all-gather.6.cloned.1.call-done = bf16[256,4096]{0,1:T(8,128)(2,1)} async-done(((bf16[256,512]{0,1:T(8,128)(2,1)}), bf16[256,4096]{0,1:T(8,128)(2,1)}) %all-gather.6.cloned.1.call-update) | async-done | bytes 2097168 | tf_op jit(solution)/shard_map/all_gather | solution.py:64
  201.9 3.2 convolution_convert_fusion.2
  205.2 10.1 %all-to-all-start = ((bf16[16,16,128]{2,1,0:T(8,128)(2,1)}), bf16[16,16,128]{2,1,0:T(8,128)(2,1)S(1)}, u32[]{:S(2)}, u32[]{:S(2)}) async-start(bf16[16,16,128]{2,1,0:T(8,128)(2,1)} %bitcast.67), calls=%async_computation | async-start | bytes 131072 | tf_op jit(solution)/shard_map/all_to_all | solution.py:258
  215.4 4.7 %all-to-all-done = bf16[16,16,128]{2,1,0:T(8,128)(2,1)S(1)} async-done(((bf16[16,16,128]{2,1,0:T(8,128)(2,1)}), bf16[16,16,128]{2,1,0:T(8,128)(2,1)S(1)}, u32[]{:S(2)}, u32[]{:S(2)}) %all-to-all-start) | async-done | bytes 65568 | tf_op jit(solution)/shard_map/all_to_all | solution.py:258
  220.3 0.3 convolution_convert_fusion.1
  220.8 21.3 %all_to_all.28 = bf16[32,2,2048]{2,1,0:T(2,128)(2,1)S(1)} all-to-all(bf16[32,2,2048]{2,1,0:T(2,128)(2,1)S(1)} %reshape.1010), channel_id=1, replica_groups=mesh['sp_0'=8,'sp_1'=4,'tp_0'=8,'tp_1'=2] {'sp_0','sp_1'}, dimensions={0} | all-to-all | bytes 524288 | tf_op jit(solution)/shard_map/all_to_all | solution.py:278
  242.1 3.2 stack.3
  245.3 102.1 %all_to_all.29 = bf16[16,1,32,2,2048]{4,3,2,1,0:T(2,128)(2,1)} all-to-all(bf16[16,1,32,2,2048]{4,3,2,1,0:T(2,128)(2,1)S(1)} %stack.3), channel_id=1, replica_groups=mesh['sp_0'=8,'sp_1'=4,'tp_0'=8,'tp_1'=2] {'tp_0','tp_1'}, dimensions={0} | all-to-all | bytes 8388608 | tf_op jit(solution)/shard_map/all_to_all | solution.py:286
  347.4 7.3 %reshape_reshape.3 = bf16[1024,2048]{1,0:T(8,128)(2,1)} reshape(bf16[16,1,32,2,2048]{4,3,2,1,0:T(2,128)(2,1)} %all_to_all.29) | data formatting | bytes 8388608 | tf_op jit(solution)/shard_map/reshape;reshape | solution.py:288
  354.7 4.5 fusion.14
  359.2 9.1 %convolution_convert_fusion = bf16[1024,2048]{1,0:T(8,128)(2,1)} fusion(bf16[1024,2048]{1,0:T(8,128)(2,1)} %reshape_reshape.3, bf16[1,256,2048]{2,1,0:T(8,128)(2,1)S(1)} %copy-done, bf16[1,2048,256]{2,1,0:T(8,128)(2,1)} %param.40, f32[1024,256]{1,0:T(8,128)} %fusion.14), kind=kOutput, calls=%fused_computation.10 | convolution fusion | flops 2151153664 | bytes 11534336 | tf_op jit(solution)/shard_map/dot_general | solution.py:292
  368.3 7.6 %convert_element_type.713 = bf16[16,32,2,2048]{3,2,1,0:T(2,128)(2,1)} reshape(bf16[1024,2048]{1,0:T(8,128)(2,1)} %convolution_convert_fusion) | data formatting | bytes 8388608 | tf_op jit(solution)/shard_map/convert_element_type | solution.py:296
  375.9 6.0 %copy.156 = bf16[16,32,2,2048]{3,1,2,0:T(8,128)(2,1)} copy(bf16[16,32,2,2048]{3,2,1,0:T(2,128)(2,1)} %convert_element_type.713) | data formatting | bytes 8388608 | tf_op jit(solution)/shard_map/convert_element_type | solution.py:296
  382.0 58.6 %reduce-scatter.2.cloned.1.call-done = bf16[1,32,2,2048]{3,1,2,0:T(8,128)(2,1)} async-done(((bf16[16,32,2,2048]{3,1,2,0:T(8,128)(2,1)}), bf16[1,32,2,2048]{3,1,2,0:T(8,128)(2,1)}) %reduce-scatter.2.cloned.1.call-update) | async-done | bytes 262160 | tf_op jit(solution)/shard_map/reduce_scatter | solution.py:295
  440.6 1.9 copy.157
  442.5 9.9 %all-to-all-start.3 = ((bf16[32,2,2048]{2,1,0:T(2,128)(2,1)}), bf16[32,2,2048]{2,1,0:T(2,128)(2,1)S(1)}, u32[]{:S(2)}, u32[]{:S(2)}) async-start(bf16[32,2,2048]{2,1,0:T(2,128)(2,1)} %copy.157), calls=%async_computation.4 | async-start | bytes 524288 | tf_op jit(solution)/shard_map/all_to_all | solution.py:302
  452.5 11.1 %all-to-all-done.3 = bf16[32,2,2048]{2,1,0:T(2,128)(2,1)S(1)} async-done(((bf16[32,2,2048]{2,1,0:T(2,128)(2,1)}), bf16[32,2,2048]{2,1,0:T(2,128)(2,1)S(1)}, u32[]{:S(2)}, u32[]{:S(2)}) %all-to-all-start.3) | async-done | bytes 262176 | tf_op jit(solution)/shard_map/all_to_all | solution.py:302
  463.8 0.8 fusion.4
  (101 shorter events, 4.5 us)
Async XLA Ops:
  6.5 352.6 %copy-start = (bf16[1,256,2048]{2,1,0:T(8,128)(2,1)S(1)}, bf16[1,256,2048]{2,1,0:T(8,128)(2,1)}, u32[]{:S(2)}) copy-start(bf16[1,256,2048]{2,1,0:T(8,128)(2,1)} %param.41) | copy-start | bytes 3145732
  6.5 195.4 %all-gather.6.cloned.1.call-start = ((), (), s32[]{:S(2)}) async-start(), calls=%async_computation.5 | async-start | bytes 2359296 | tf_op jit(solution)/shard_map/all_gather | solution.py:64
  9.7 54.5 %collective-permute-start = (bf16[2,512]{0,1:T(8,128)(2,1)S(1)}, bf16[2,512]{0,1:T(8,128)(2,1)S(1)}, u32[]{:S(2)}, u32[]{:S(2)}) collective-permute-start(bf16[2,512]{0,1:T(8,128)(2,1)S(1)} %get-tuple-element.275), channel_id=1, source_target_pairs={{0,16},{16,32},{32,48},{48,64},{64,80},{80,96},{96,112},{112,128},... | collective-permute-start | bytes 6152 | tf_op jit(solution)/shard_map/ppermute | solution.py:25
  12.8 51.4 %collective-permute-start.1 = (bf16[2,512]{0,1:T(8,128)(2,1)S(1)}, bf16[2,512]{0,1:T(8,128)(2,1)S(1)}, u32[]{:S(2)}, u32[]{:S(2)}) collective-permute-start(bf16[2,512]{0,1:T(8,128)(2,1)S(1)} %get-tuple-element.276), channel_id=1, source_target_pairs={{16,0},{32,16},{48,32},{64,48},{80,64},{96,80},{112,96},{128,112},... | collective-permute-start | bytes 6152 | tf_op jit(solution)/shard_map/ppermute | solution.py:27
  17.8 46.2 %copy-start.5 = (f32[2,4]{1,0:T(2,128)}, f32[2,4]{1,0:T(2,128)S(1)}, u32[]{:S(2)}) copy-start(f32[2,4]{1,0:T(2,128)S(1)} %get-tuple-element.240) | copy-start | bytes 100
  62.3 14.6 %copy-start.7 = (f32[4]{0:T(128)}, f32[4]{0:T(128)S(1)}, u32[]{:S(2)}) copy-start(f32[4]{0:T(128)S(1)} %get-tuple-element.308) | copy-start | bytes 52
  62.3 14.6 %copy-start.8 = (f32[4]{0:T(128)}, f32[4]{0:T(128)S(1)}, u32[]{:S(2)}) copy-start(f32[4]{0:T(128)S(1)} %get-tuple-element.309) | copy-start | bytes 52
  62.3 14.6 %copy-start.9 = (f32[4]{0:T(128)}, f32[4]{0:T(128)S(1)}, u32[]{:S(2)}) copy-start(f32[4]{0:T(128)S(1)} %get-tuple-element.310) | copy-start | bytes 52
  62.3 14.6 %copy-start.10 = (f32[4]{0:T(128)}, f32[4]{0:T(128)S(1)}, u32[]{:S(2)}) copy-start(f32[4]{0:T(128)S(1)} %get-tuple-element.311) | copy-start | bytes 52
  66.5 0.7 copy-start.2
  67.2 40.7 %copy-start.11 = (f32[4]{0:T(128)S(1)}, f32[4]{0:T(128)}, u32[]{:S(2)}) copy-start(f32[4]{0:T(128)} %get-tuple-element.313) | copy-start | bytes 52
  67.2 40.7 %copy-start.12 = (f32[4]{0:T(128)S(1)}, f32[4]{0:T(128)}, u32[]{:S(2)}) copy-start(f32[4]{0:T(128)} %get-tuple-element.314) | copy-start | bytes 52
  67.2 40.7 %copy-start.13 = (f32[4]{0:T(128)S(1)}, f32[4]{0:T(128)}, u32[]{:S(2)}) copy-start(f32[4]{0:T(128)} %get-tuple-element.315) | copy-start | bytes 52
  67.2 40.7 %copy-start.14 = (f32[4]{0:T(128)S(1)}, f32[4]{0:T(128)}, u32[]{:S(2)}) copy-start(f32[4]{0:T(128)} %get-tuple-element.316) | copy-start | bytes 52
  67.5 29.1 %copy-start.1 = (f32[2,1,4,64,128]{4,3,2,1,0:T(8,128)}, f32[2,1,4,64,128]{4,3,2,1,0:T(8,128)S(1)}, u32[]{:S(2)}) copy-start(f32[2,1,4,64,128]{4,3,2,1,0:T(8,128)S(1)} %get-tuple-element.138) | copy-start | bytes 786436
  96.2 11.7 %copy-start.3 = (bf16[2,128,4,64]{1,0,3,2:T(2,128)(2,1)}, bf16[2,128,4,64]{1,0,3,2:T(2,128)(2,1)S(1)}, u32[]{:S(2)}) copy-start(bf16[2,128,4,64]{1,0,3,2:T(2,128)(2,1)S(1)} %reshape.1005) | copy-start | bytes 393220
  132.7 87.4 %copy-start.4 = (bf16[16,2048]{1,0:T(8,128)(2,1)S(1)}, bf16[16,2048]{1,0:T(8,128)(2,1)}, u32[]{:S(2)}) copy-start(bf16[16,2048]{1,0:T(8,128)(2,1)} %param.23) | copy-start | bytes 196612
  132.8 87.6 %copy-start.6 = (f32[2048]{0:T(1024)S(1)}, f32[2048]{0:T(1024)}, u32[]{:S(2)}) copy-start(f32[2048]{0:T(1024)} %param.36) | copy-start | bytes 24580
  205.2 15.0 %all-to-all-start = ((bf16[16,16,128]{2,1,0:T(8,128)(2,1)}), bf16[16,16,128]{2,1,0:T(8,128)(2,1)S(1)}, u32[]{:S(2)}, u32[]{:S(2)}) async-start(bf16[16,16,128]{2,1,0:T(8,128)(2,1)} %bitcast.67), calls=%async_computation | async-start | bytes 131072 | tf_op jit(solution)/shard_map/all_to_all | solution.py:258
  215.2 225.4 %reduce-scatter.2.cloned.1.call-start = ((), (), s32[]{:S(2)}) async-start(), calls=%async_computation.6 | async-start | bytes 4456448 | tf_op jit(solution)/shard_map/reduce_scatter | solution.py:295
  347.4 7.3 %copy-start.16 = (bf16[1,2048,256]{2,1,0:T(8,128)(2,1)S(1)}, bf16[1,2048,256]{2,1,0:T(8,128)(2,1)}, u32[]{:S(2)}) copy-start(bf16[1,2048,256]{2,1,0:T(8,128)(2,1)} %param.39) | copy-start | bytes 3145732
  381.9 70.5 %copy-start.15 = (f32[16,2]{0,1:T(2,128)S(1)}, f32[16,2]{0,1:T(2,128)}, u32[]{:S(2)}) copy-start(f32[16,2]{0,1:T(2,128)} %param.38) | copy-start | bytes 388
  442.5 21.1 %all-to-all-start.3 = ((bf16[32,2,2048]{2,1,0:T(2,128)(2,1)}), bf16[32,2,2048]{2,1,0:T(2,128)(2,1)S(1)}, u32[]{:S(2)}, u32[]{:S(2)}) async-start(bf16[32,2,2048]{2,1,0:T(2,128)(2,1)} %copy.157), calls=%async_computation.4 | async-start | bytes 524288 | tf_op jit(solution)/shard_map/all_to_all | solution.py:302
Sparse Core Ops, SparseCore 0:
  167.2 34.6 all-gather.5
  382.1 58.4 reduce-scatter.1
